TPU v7x, 32 devices: a whole 2x2x4 slice. The times are simulated.
32 devices in a mesh: sp: 8 (over z, y), tp: 4 (over x, core).
Axes of the slice: x: 2, y: 2, z: 4, core: 2. Of those that a mesh axis runs over, the one named last changes fastest.
Arguments:
- out_grad: bfloat16 [1024, 2048], P('sp', 'tp'), may hold values from -6 to 6
- route_ids: int32 [1024, 2], P('sp'), may hold values from 0 to 7, as said below
- route_weight: float32 [1024, 2], P('sp'), may hold values from 0.1 to 0.9
- expert_inputs: bfloat16 [8, 512, 2048], P('sp'), may hold values from -6 to 6
- gate_weight: bfloat16 [8, 2048, 3072], P('sp', None, 'tp'), may hold values from -0.125 to 0.125
- up_weight: bfloat16 [8, 2048, 3072], P('sp', None, 'tp'), may hold values from -0.125 to 0.125
- down_weight: bfloat16 [8, 3072, 2048], P('sp', 'tp'), may hold values from -0.109375 to 0.109375
- out_gate: bfloat16 [1024, 2048], P('sp', 'tp'), may hold values from -6 to 6
- in_gate: bfloat16 [1024, 2048], P('sp', 'tp'), may hold values from -6 to 6
- values: bfloat16 [1024, 2048], P('sp', 'tp'), may hold values from -6 to 6
- conv_out: bfloat16 [1024, 2048], P('sp', 'tp'), may hold values from -6 to 6
- conv_taps: bfloat16 [3, 2048], P(None, 'tp'), may hold values from -3.5 to 3.5
- proj_weight: bfloat16 [2048, 2048], P(None, 'tp'), may hold values from -0.125 to 0.125
Outputs:
- resid_grad: bfloat16 [1024, 2048], P('sp', 'tp')
- out_gate_grad: bfloat16 [1024, 2048], P('sp', 'tp')
- in_gate_grad: bfloat16 [1024, 2048], P('sp', 'tp')
- values_grad: bfloat16 [1024, 2048], P('sp', 'tp')
- proj_grad: float32 [2048, 2048], P('sp', 'tp')
- gate_grad: bfloat16 [8, 2048, 3072], P('sp', None, 'tp')
- up_grad: bfloat16 [8, 2048, 3072], P('sp', None, 'tp')
- down_grad: bfloat16 [8, 3072, 2048], P('sp', 'tp')
Inputs may be any that keep to these rules, and one draw needn't show every extreme that they name: `route_ids`: each row names two different experts. Among the rows of one device (aligned blocks of 128 rows) no expert is named more than 64 times, and in every draw one expert is named exactly 64 times in every block.
All inputs are finite; a program needn't handle non-finite values.
Results may differ from a plain program's by a relative error of at most 0.017.
Values may be sent and summed in bfloat16 or wider, within the bound.
A program may use at most 128 MiB of HBM per device.

v0:
```python
import math
import jax
import jax.numpy as jnp
from jax import lax
from jax.sharding import PartitionSpec as P


def extended(x, sides, width):
    for axis, dim in sides:
        devices, length = (lax.axis_size(axis), x.shape[dim])
        up = [(i, (i + 1) % devices) for i in range(devices - 1)]
        down = [(j, i) for i, j in up]
        last = lax.slice_in_dim(x, length - width, length, axis=dim)
        first = lax.slice_in_dim(x, 0, width, axis=dim)
        before = lax.ppermute(last, axis, up)
        after = lax.ppermute(first, axis, down)
        x = jnp.concatenate([before, x, after], axis=dim)
    return x


def contract_first(left, right):
    return lax.dot_general(
        left, right, (((0,), (0,)), ((), ())), preferred_element_type=jnp.float32
    )


def contract_last(left, right):
    return lax.dot_general(
        left, right, (((1,), (1,)), ((), ())), preferred_element_type=jnp.float32
    )


def expert_backward(inputs, routed, gate_w, up_w, down_w):
    pre_gate = jnp.dot(inputs, gate_w, preferred_element_type=jnp.float32)
    pre_up = jnp.dot(inputs, up_w, preferred_element_type=jnp.float32)
    sigmoid_g = jax.nn.sigmoid(pre_gate)
    activated = pre_gate * sigmoid_g
    hidden = (activated * pre_up).astype(jnp.bfloat16)
    d_hidden = contract_last(routed, down_w)
    d_gate = (d_hidden * pre_up * sigmoid_g * (1.0 + pre_gate * (1.0 - sigmoid_g))).astype(
        jnp.bfloat16
    )
    d_up = (d_hidden * activated).astype(jnp.bfloat16)
    partial_value = contract_last(d_gate, gate_w) + contract_last(d_up, up_w)
    grad_set = (
        contract_first(inputs, d_gate),
        contract_first(inputs, d_up),
        contract_first(hidden, routed),
    )
    return (partial_value, grad_set)


def expert_pass(outgoing, input_rows, gate_weight, up_weight, down_weight):
    arrived = lax.all_to_all(outgoing, "sp", split_axis=0, concat_axis=1, tiled=True)
    routed = lax.all_gather(arrived, "tp", axis=2, tiled=True)
    partial_value, grad_set = expert_backward(
        input_rows[0], routed[0], gate_weight[0], up_weight[0], down_weight[0]
    )
    partials = [partial_value]
    gate_list = [grad_set[0]]
    up_list = [grad_set[1]]
    down_list = [grad_set[2]]
    summed = lax.psum_scatter(
        jnp.stack(partials).astype(jnp.bfloat16), "tp", scatter_dimension=2, tiled=True
    )
    returned = lax.all_to_all(summed, "sp", split_axis=1, concat_axis=0, tiled=True)
    return (returned, (jnp.stack(gate_list), jnp.stack(up_list), jnp.stack(down_list)))


def per_device(
    out_grad,
    route_ids,
    route_weight,
    expert_inputs,
    gate_weight,
    up_weight,
    down_weight,
    out_gate,
    in_gate,
    values,
    conv_out,
    conv_taps,
    proj_weight,
):
    sp_devices = lax.axis_size("sp")
    tok_rows = out_grad.shape[0]
    local_experts = gate_weight.shape[0]
    all_experts = sp_devices * local_experts
    capacity = 4 * tok_rows // all_experts
    flat_ids = route_ids.reshape(-1)
    onehot = (flat_ids[:, None] == jnp.arange(all_experts, dtype=jnp.int32)[None, :]).astype(
        jnp.int32
    )
    ranked = jnp.sum((jnp.cumsum(onehot, axis=0) - onehot) * onehot, axis=1)
    slot_ids = flat_ids * capacity + ranked
    dispatch = (
        jnp.arange(all_experts * capacity, dtype=jnp.int32)[:, None] == slot_ids[None, :]
    ).astype(jnp.bfloat16)
    weighted = (
        (route_weight[:, :, None] * out_grad.astype(jnp.float32)[:, None, :])
        .astype(jnp.bfloat16)
        .reshape(2 * tok_rows, -1)
    )
    outgoing = jnp.dot(dispatch, weighted, preferred_element_type=jnp.float32).astype(jnp.bfloat16)
    outgoing = outgoing.reshape(all_experts, capacity, -1)
    returned, totals = expert_pass(outgoing, expert_inputs, gate_weight, up_weight, down_weight)
    slot_scale = 1.0 / math.sqrt(expert_inputs.shape[1])
    gate_grad = (totals[0] * slot_scale).astype(jnp.bfloat16)
    up_grad = (totals[1] * slot_scale).astype(jnp.bfloat16)
    down_grad = (totals[2] * slot_scale).astype(jnp.bfloat16)
    combiner = jnp.sum(dispatch.reshape(all_experts * capacity, tok_rows, 2), axis=2)
    moe_part = contract_first(combiner, returned.reshape(all_experts * capacity, -1))
    resid_grad = (out_grad.astype(jnp.float32) + moe_part).astype(jnp.bfloat16)
    resid_full = lax.all_gather(resid_grad, "tp", axis=1, tiled=True)
    mix_grad = jnp.dot(resid_full, proj_weight, preferred_element_type=jnp.float32)
    gate_vals = out_gate.astype(jnp.float32)
    conv_vals = conv_out.astype(jnp.float32)
    mixed_in = (gate_vals * conv_vals).astype(jnp.bfloat16)
    out_gate_grad = (mix_grad * conv_vals).astype(jnp.bfloat16)
    conv_grad = (mix_grad * gate_vals).astype(jnp.bfloat16)
    padded = extended(conv_grad, (("sp", 0),), 1).astype(jnp.float32)
    tap_vals = conv_taps.astype(jnp.float32)
    value_grad = padded[2:] * tap_vals[0] + padded[1:-1] * tap_vals[1] + padded[:-2] * tap_vals[2]
    in_gate_grad = (value_grad * values.astype(jnp.float32)).astype(jnp.bfloat16)
    values_grad = (value_grad * in_gate.astype(jnp.float32)).astype(jnp.bfloat16)
    token_scale = 1.0 / math.sqrt(tok_rows * sp_devices)
    columns = lax.all_to_all(resid_full, "sp", split_axis=1, concat_axis=0, tiled=True)
    proj_sum = contract_first(columns, lax.all_gather(mixed_in, "sp", axis=0, tiled=True))
    proj_grad = proj_sum * token_scale
    return (
        resid_grad,
        out_gate_grad,
        in_gate_grad,
        values_grad,
        proj_grad,
        gate_grad,
        up_grad,
        down_grad,
    )


def solution(mesh):
    in_specs = (
        P("sp", "tp"),
        P("sp", None),
        P("sp", None),
        P("sp", None, None),
        P("sp", None, "tp"),
        P("sp", None, "tp"),
        P("sp", "tp", None),
        P("sp", "tp"),
        P("sp", "tp"),
        P("sp", "tp"),
        P("sp", "tp"),
        P(None, "tp"),
        P(None, "tp"),
    )
    out_specs = (
        P("sp", "tp"),
        P("sp", "tp"),
        P("sp", "tp"),
        P("sp", "tp"),
        P("sp", "tp"),
        P("sp", None, "tp"),
        P("sp", None, "tp"),
        P("sp", "tp", None),
    )
    return jax.shard_map(
        per_device, mesh=mesh, in_specs=in_specs, out_specs=out_specs, check_vma=False
    )
```

profile of v0, /device:TPU:0, one launch (start us, length us, event | category | flops | bytes accessed | tf_op | source)
XLA Modules:
  0.0 198.5 jit_solution(15342331069827276)
XLA Ops:
  7.2 0.0 copy-start
  7.2 0.0 all-gather.3.cloned.1.call-start
  7.2 0.9 copy.60
  8.2 0.1 eq.50
  8.3 0.1 eq.46
  8.5 0.6 reduce-window.6
  9.0 0.2 slice_reduce_fusion
  9.3 0.1 fusion.39
  9.4 1.8 mul.130
  11.2 2.2 %mul.131 = f32[256,512]{1,0:T(8,128)} reshape(f32[128,2,512]{2,1,0:T(2,128)} %mul.130) | data formatting | bytes 1048576 | tf_op jit(solution)/shard_map/mul | solution.py:100
  13.4 0.8 copy.63
  14.2 0.1 mul.128
  14.4 1.4 convolution_convert_fusion
  15.8 21.7 %all_to_all.40 = bf16[8,64,512]{2,1,0:T(8,128)(2,1)} all-to-all(bf16[8,64,512]{2,1,0:T(8,128)(2,1)S(1)} %bitcast.88), channel_id=1, replica_groups=mesh['sp'=8,'tp'=4] {'sp'}, dimensions={0} | all-to-all | bytes 1048576 | tf_op jit(solution)/shard_map/all_to_all | solution.py:54
  37.5 0.0 all-gather.3.cloned.1.call-update
  37.6 0.0 reduce-scatter.2.cloned.1.call-start
  37.6 0.0 copy-start.9
  37.6 0.0 copy-start.11
  37.6 4.7 %fusion.2 = f32[512,768]{1,0:T(8,128)} fusion(bf16[1,2048,768]{2,1,0:T(8,128)(2,1)S(1)} %copy-done, bf16[1,512,2048]{2,1,0:T(8,128)(2,1)} %param.16), kind=kOutput, calls=%fused_computation.6 | convolution fusion | flops 1610612736 | bytes 6815744 | tf_op jit(solution)/shard_map/dot_general | solution.py:34
  42.3 3.0 %fusion.6 = f32[512,768]{1,0:T(8,128)} fusion(bf16[1,2048,768]{2,1,0:T(8,128)(2,1)S(1)} %copy-done.9, bf16[1,512,2048]{2,1,0:T(8,128)(2,1)S(1)} %copy-done.11), kind=kOutput, calls=%fused_computation.10 | convolution fusion | flops 1610612736 | bytes 6815744 | tf_op jit(solution)/shard_map/dot_general | solution.py:35
  45.3 14.0 %all-gather.3.cloned.1.call-done = bf16[1,512,2048]{2,1,0:T(8,128)(2,1)} async-done(((bf16[1,512,512]{2,1,0:T(8,128)(2,1)}), bf16[1,512,2048]{2,1,0:T(8,128)(2,1)}) %all-gather.3.cloned.1.call-update) | async-done | bytes 2097168 | tf_op jit(solution)/shard_map/all_gather | solution.py:55
  59.3 5.6 %multiply_convert_fusion.4 = (bf16[512,768]{1,0:T(8,128)(2,1)S(1)}, bf16[512,768]{1,0:T(8,128)(2,1)S(1)}) fusion(f32[512,768]{1,0:T(8,128)} %fusion.2, f32[512,768]{1,0:T(8,128)} %fusion.6, bf16[1,768,2048]{2,1,0:T(8,128)(2,1)} %param.19, bf16[1,512,2048]{2,1,0:T(8,128)(2,1)} %all-gather.3.cloned.1.call-done), kind=kOutput, calls=%fused_computation.25 | convolution fusion | flops 1615724544 | bytes 9961472 | tf_op jit(solution)/shard_map/dot_general | solution.py:28
  64.9 0.0 copy-start.10
  65.0 1.8 fusion
  66.8 0.6 copy-done.10
  67.4 3.1 %fusion.15 = bf16[1,512,2048]{2,1,0:T(8,128)(2,1)} fusion(f32[512,2048]{1,0:T(8,128)S(1)} %fusion, bf16[512,768]{1,0:T(8,128)(2,1)S(1)} %get-tuple-element.58, bf16[1,2048,768]{2,1,0:T(8,128)(2,1)S(1)} %copy-done.10), kind=kOutput, calls=%fused_computation.17 | convolution fusion | flops 1612709888 | bytes 10223616 | tf_op jit(solution)/shard_map/dot_general | solution.py:28
  70.5 0.0 reduce-scatter.2.cloned.1.call-update
  70.6 0.1 reduce_sum.24
  70.7 0.1 copy.62
  70.8 31.1 %reduce-scatter.2.cloned.1.call-done = bf16[1,512,512]{2,1,0:T(8,128)(2,1)} async-done(((bf16[1,512,2048]{2,1,0:T(8,128)(2,1)}), bf16[1,512,512]{2,1,0:T(8,128)(2,1)}) %reduce-scatter.2.cloned.1.call-update) | async-done | bytes 524304 | tf_op jit(solution)/shard_map/reduce_scatter | solution.py:63
  101.9 2.8 %copy.77 = bf16[1,512,512]{2,0,1:T(2,128)(2,1)} copy(bf16[1,512,512]{2,1,0:T(8,128)(2,1)} %reduce-scatter.2.cloned.1.call-done) | data formatting | bytes 1048576 | tf_op jit(solution)/shard_map/reduce_scatter | solution.py:63
  104.7 0.5 broadcast.62
  105.2 5.6 %reduce.3 = bf16[512,512]{1,0:T(8,128)(2,1)} reduce(bf16[512,1,512]{2,1,0:T(2,128)(2,1)} %bitcast.84, bf16[]{:T(256)} %broadcast.62), dimensions={1}, to_apply=%bitcast.82.reduce_sub_computation | reduce | bytes 1048578
  110.8 2.2 %reshape.85 = bf16[8,2,16384]{2,1,0:T(2,128)(2,1)} reshape(bf16[512,512]{1,0:T(8,128)(2,1)} %reduce.3) | data formatting | bytes 1048576
  113.0 5.5 %all-to-all-start.1 = ((bf16[8,2,16384]{2,1,0:T(2,128)(2,1)}), bf16[8,2,16384]{2,1,0:T(2,128)(2,1)}, u32[]{:S(2)}, u32[]{:S(2)}) async-start(bf16[8,2,16384]{2,1,0:T(2,128)(2,1)} %reshape.85), calls=%async_computation.2 | async-start | bytes 1048576 | tf_op jit(solution)/shard_map/all_to_all | solution.py:66
  118.5 0.2 all-gather.5.cloned.1.call-start
  118.8 0.1 fusion.33
  118.8 0.0 copy-start.3
  118.9 5.4 %fusion.10 = bf16[1,2048,768]{1,2,0:T(8,128)(2,1)} fusion(bf16[512,768]{1,0:T(8,128)(2,1)} %copy-done.13, bf16[1,512,2048]{2,1,0:T(8,128)(2,1)} %param.16), kind=kOutput, calls=%fused_computation.14 | convolution fusion | flops 1613758464 | bytes 6029312 | tf_op jit(solution)/shard_map/dot_general | solution.py:22
  124.2 8.7 %all-to-all-done.1 = bf16[8,2,16384]{2,1,0:T(2,128)(2,1)} async-done(((bf16[8,2,16384]{2,1,0:T(2,128)(2,1)}), bf16[8,2,16384]{2,1,0:T(2,128)(2,1)}, u32[]{:S(2)}, u32[]{:S(2)}) %all-to-all-start.1) | async-done | bytes 524320 | tf_op jit(solution)/shard_map/all_to_all | solution.py:66
  132.9 3.5 %reshape.86 = bf16[512,1,512]{2,1,0:T(2,128)(2,1)} reshape(bf16[8,2,16384]{2,1,0:T(2,128)(2,1)} %all-to-all-done.1) | data formatting | bytes 1048576
  136.4 1.5 fusion.25
  137.9 0.0 copy-start.4
  137.9 6.5 %all_gather.10 = bf16[128,2048]{1,0:T(8,128)(2,1)S(1)} all-gather(bf16[128,512]{1,0:T(8,128)(2,1)S(1)} %fusion.25), channel_id=1, replica_groups=mesh['sp'=8,'tp'=4] {'tp'}, dimensions={1}, use_global_device_ids=true | all-gather | bytes 655360 | tf_op jit(solution)/shard_map/all_gather | solution.py:114
  144.4 0.8 copy-done.1
  145.2 2.8 %fusion.31 = (bf16[128,512]{1,0:T(8,128)(2,1)S(1)}, bf16[128,512]{1,0:T(8,128)(2,1)}, bf16[128,512]{1,0:T(8,128)(2,1)}) fusion(bf16[128,512]{1,0:T(8,128)(2,1)} %param.20, bf16[128,512]{1,0:T(8,128)(2,1)} %param.23, bf16[128,2048]{1,0:T(8,128)(2,1)S(1)} %all_gather.10, bf16[2048,512]{1,0:T(8,128)(2,1)} %param.25), kind=kOutput, calls=%fused_computation.44 | convolution fusion | flops 268959744 | bytes 3276800 | tf_op jit(solution)/shard_map/dot_general | solution.py:115
  148.0 0.0 all-gather.5.cloned.1.call-update
  148.0 0.0 copy-start.2
  148.0 6.1 %fusion.12 = bf16[1,768,2048]{2,1,0:T(8,128)(2,1)} fusion(bf16[1,512,2048]{2,1,0:T(8,128)(2,1)} %all-gather.3.cloned.1.call-done, f32[512,768]{1,0:T(8,128)} %fusion.6, f32[512,768]{1,0:T(8,128)} %fusion.2), kind=kOutput, calls=%fused_computation.16 | convolution fusion | flops 1616117760 | bytes 8388608 | tf_op jit(solution)/shard_map/dot_general | solution.py:22
  154.2 0.6 fusion.43
  154.8 3.4 %collective-permute-start = (bf16[1,512]{1,0:T(2,128)(2,1)}, bf16[1,512]{1,0:T(2,128)(2,1)S(1)}, u32[]{:S(2)}, u32[]{:S(2)}) collective-permute-start(bf16[1,512]{1,0:T(2,128)(2,1)} %get-tuple-element.63), channel_id=1, source_target_pairs={{0,4},{4,8},{8,12},{12,16},{16,20},{20,24},{24,28},{1,5},{5,9},{9,... | collective-permute-start | bytes 3080 | tf_op jit(solution)/shard_map/ppermute | solution.py:15
  158.1 1.3 collective-permute-start.1
  159.4 0.8 copy.76
  160.3 5.8 %all-to-all-start.2 = ((bf16[128,8,256]{2,0,1:T(8,128)(2,1)}), bf16[128,8,256]{2,0,1:T(8,128)(2,1)}, u32[]{:S(2)}, u32[]{:S(2)}) async-start(bf16[128,8,256]{2,0,1:T(8,128)(2,1)} %bitcast.86), calls=%async_computation.3 | async-start | bytes 1048576 | tf_op jit(solution)/shard_map/all_to_all | solution.py:127
  166.0 5.3 %fusion.11 = bf16[1,2048,768]{1,2,0:T(8,128)(2,1)} fusion(bf16[512,768]{1,0:T(8,128)(2,1)} %copy-done.12, bf16[1,512,2048]{2,1,0:T(8,128)(2,1)} %param.16), kind=kOutput, calls=%fused_computation.15 | convolution fusion | flops 1613758464 | bytes 6029312 | tf_op jit(solution)/shard_map/dot_general | solution.py:22
  171.3 4.6 %copy.66 = bf16[1,2048,768]{2,1,0:T(8,128)(2,1)} copy(bf16[1,2048,768]{1,2,0:T(8,128)(2,1)} %fusion.10) | data formatting | bytes 6291456
  176.0 4.7 %copy.67 = bf16[1,2048,768]{2,1,0:T(8,128)(2,1)} copy(bf16[1,2048,768]{1,2,0:T(8,128)(2,1)} %fusion.11) | data formatting | bytes 6291456
  180.6 0.0 collective-permute-done
  180.6 0.7 maximum_convert_fusion
  181.4 0.8 multiply_convert_fusion.9
  182.1 0.7 multiply_convert_fusion.10
  182.8 5.7 %all-to-all-done.2 = bf16[128,8,256]{2,0,1:T(8,128)(2,1)} async-done(((bf16[128,8,256]{2,0,1:T(8,128)(2,1)}), bf16[128,8,256]{2,0,1:T(8,128)(2,1)}, u32[]{:S(2)}, u32[]{:S(2)}) %all-to-all-start.2) | async-done | bytes 524320 | tf_op jit(solution)/shard_map/all_to_all | solution.py:127
  188.5 0.8 all-gather.5.cloned.1.call-done
  189.3 2.6 %convolution_multiply_fusion = f32[256,512]{1,0:T(8,128)} fusion(bf16[1024,256]{1,0:T(8,128)(2,1)} %bitcast.14, bf16[1024,512]{1,0:T(8,128)(2,1)} %all-gather.5.cloned.1.call-done), kind=kOutput, calls=%fused_computation.30 | convolution fusion | flops 268566528 | bytes 2097152 | tf_op jit(solution)/shard_map/dot_general | solution.py:22
  (26 shorter events, 0.1 us)
Async XLA Ops:
  7.2 30.4 %copy-start = (bf16[1,2048,768]{2,1,0:T(8,128)(2,1)S(1)}, bf16[1,2048,768]{2,1,0:T(8,128)(2,1)}, u32[]{:S(2)}) copy-start(bf16[1,2048,768]{2,1,0:T(8,128)(2,1)} %param.17) | copy-start | bytes 9437188
  7.2 52.1 %all-gather.3.cloned.1.call-start = ((), (), s32[]{:S(2)}) async-start(), calls=%async_computation.4 | async-start | bytes 2621440 | tf_op jit(solution)/shard_map/all_gather | solution.py:55
  37.6 64.3 %reduce-scatter.2.cloned.1.call-start = ((), (), s32[]{:S(2)}) async-start(), calls=%async_computation.5 | async-start | bytes 2621440 | tf_op jit(solution)/shard_map/reduce_scatter | solution.py:63
  37.6 4.7 %copy-start.9 = (bf16[1,2048,768]{2,1,0:T(8,128)(2,1)S(1)}, bf16[1,2048,768]{2,1,0:T(8,128)(2,1)}, u32[]{:S(2)}) copy-start(bf16[1,2048,768]{2,1,0:T(8,128)(2,1)} %param.18) | copy-start | bytes 9437188
  37.6 4.7 %copy-start.11 = (bf16[1,512,2048]{2,1,0:T(8,128)(2,1)S(1)}, bf16[1,512,2048]{2,1,0:T(8,128)(2,1)}, u32[]{:S(2)}) copy-start(bf16[1,512,2048]{2,1,0:T(8,128)(2,1)} %param.16) | copy-start | bytes 6291460
  64.9 1.9 copy-start.13
  64.9 1.9 copy-start.12
  64.9 2.5 %copy-start.10 = (bf16[1,2048,768]{2,1,0:T(8,128)(2,1)S(1)}, bf16[1,2048,768]{2,1,0:T(8,128)(2,1)}, u32[]{:S(2)}) copy-start(bf16[1,2048,768]{2,1,0:T(8,128)(2,1)} %param.18) | copy-start | bytes 9437188
  104.7 14.0 %copy-start.8 = (s32[128,2]{0,1:T(2,128)S(1)}, s32[128,2]{0,1:T(2,128)}, u32[]{:S(2)}) copy-start(s32[128,2]{0,1:T(2,128)} %param.14) | copy-start | bytes 3076
  104.7 14.1 %copy-start.7 = (bf16[3,512]{1,0:T(4,128)(2,1)S(1)}, bf16[3,512]{1,0:T(4,128)(2,1)}, u32[]{:S(2)}) copy-start(bf16[3,512]{1,0:T(4,128)(2,1)} %param.24) | copy-start | bytes 9220
  113.0 19.9 %all-to-all-start.1 = ((bf16[8,2,16384]{2,1,0:T(2,128)(2,1)}), bf16[8,2,16384]{2,1,0:T(2,128)(2,1)}, u32[]{:S(2)}, u32[]{:S(2)}) async-start(bf16[8,2,16384]{2,1,0:T(2,128)(2,1)} %reshape.85), calls=%async_computation.2 | async-start | bytes 1048576 | tf_op jit(solution)/shard_map/all_to_all | solution.py:66
  118.5 70.8 %all-gather.5.cloned.1.call-start = ((), (), s32[]{:S(2)}) async-start(), calls=%async_computation.6 | async-start | bytes 1179648 | tf_op jit(solution)/shard_map/all_gather | solution.py:128
  118.8 17.6 %copy-start.3 = (bf16[128,512]{1,0:T(8,128)(2,1)S(1)}, bf16[128,512]{1,0:T(8,128)(2,1)}, u32[]{:S(2)}) copy-start(bf16[128,512]{1,0:T(8,128)(2,1)} %param.13) | copy-start | bytes 393220
  137.9 16.3 %copy-start.4 = (bf16[128,512]{1,0:T(8,128)(2,1)}, bf16[128,512]{1,0:T(8,128)(2,1)S(1)}, u32[]{:S(2)}) copy-start(bf16[128,512]{1,0:T(8,128)(2,1)S(1)} %fusion.25) | copy-start | bytes 393220
  144.4 0.8 copy-start.1
  148.0 11.4 %copy-start.2 = (bf16[128,2048]{1,0:T(8,128)(2,1)S(1)}, bf16[128,2048]{1,0:T(8,128)(2,1)}, u32[]{:S(2)}) copy-start(bf16[128,2048]{1,0:T(8,128)(2,1)} %copy-done.1) | copy-start | bytes 1572868
  154.8 25.9 %collective-permute-start = (bf16[1,512]{1,0:T(2,128)(2,1)}, bf16[1,512]{1,0:T(2,128)(2,1)S(1)}, u32[]{:S(2)}, u32[]{:S(2)}) collective-permute-start(bf16[1,512]{1,0:T(2,128)(2,1)} %get-tuple-element.63), channel_id=1, source_target_pairs={{0,4},{4,8},{8,12},{12,16},{16,20},{20,24},{24,28},{1,5},{5,9},{9,... | collective-permute-start | bytes 3080 | tf_op jit(solution)/shard_map/ppermute | solution.py:15
  158.1 22.5 %collective-permute-start.1 = (bf16[1,512]{1,0:T(2,128)(2,1)}, bf16[1,512]{1,0:T(2,128)(2,1)}, u32[]{:S(2)}, u32[]{:S(2)}) collective-permute-start(bf16[1,512]{1,0:T(2,128)(2,1)} %get-tuple-element.64), channel_id=1, source_target_pairs={{4,0},{8,4},{12,8},{16,12},{20,16},{24,20},{28,24},{5,1},{9,5},{13... | collective-permute-start | bytes 3080 | tf_op jit(solution)/shard_map/ppermute | solution.py:16
  160.3 28.2 %all-to-all-start.2 = ((bf16[128,8,256]{2,0,1:T(8,128)(2,1)}), bf16[128,8,256]{2,0,1:T(8,128)(2,1)}, u32[]{:S(2)}, u32[]{:S(2)}) async-start(bf16[128,8,256]{2,0,1:T(8,128)(2,1)} %bitcast.86), calls=%async_computation.3 | async-start | bytes 1048576 | tf_op jit(solution)/shard_map/all_to_all | solution.py:127
  176.0 5.4 %copy-start.5 = (bf16[128,512]{1,0:T(8,128)(2,1)S(1)}, bf16[128,512]{1,0:T(8,128)(2,1)}, u32[]{:S(2)}) copy-start(bf16[128,512]{1,0:T(8,128)(2,1)} %param.21) | copy-start | bytes 393220
  176.0 6.2 %copy-start.6 = (bf16[128,512]{1,0:T(8,128)(2,1)S(1)}, bf16[128,512]{1,0:T(8,128)(2,1)}, u32[]{:S(2)}) copy-start(bf16[128,512]{1,0:T(8,128)(2,1)} %param.22) | copy-start | bytes 393220
Sparse Core Ops, SparseCore 0:
  37.7 21.5 all-gather.2
  70.7 31.1 reduce-scatter.1
  148.1 41.1 all-gather.4
where the time goes:
time: 200 us; the launch traced here: 198 us
  waiting for transfers between devices  60.4 us (30%)
  matrix products  43.4 us (22%)
  blocking collectives  28.2 us (14%)
  local copies, waits for them, and re-layouts  27.8 us (14%)
  starting transfers between devices  16.2 us (8%)
  between operations  14 us (7%)
  other arithmetic  8.51 us (4%)
    reduce_scatter x1, waiting for transfers between devices, expert_pass(): lax.psum_scatter(jnp.stack(partials).astype(jnp.bfloat16), 'tp', scatter_...  31.1 us
    all_to_all x1, blocking collectives, expert_pass(): lax.all_to_all(outgoing, 'sp', split_axis=0, concat_axis=1, tiled=True)  21.7 us
    dot_general x5, matrix products, contract_first(): lax.dot_general(left, right, (((0,), (0,)), ((), ())), preferred_element_...  20.9 us
    unnamed x35, local copies, waits for them, and re-layouts  18.7 us
    all_gather x1, waiting for transfers between devices, expert_pass(): routed = lax.all_gather(arrived, 'tp', axis=2, tiled=True)  14 us
    dot_general x3, matrix products, contract_last(): lax.dot_general(left, right, (((1,), (1,)), ((), ())), preferred_element_...  10.6 us
    all_to_all x1, waiting for transfers between devices, expert_pass(): lax.all_to_all(summed, 'sp', split_axis=1, concat_axis=0, tiled=True)  8.71 us
    all_gather x1, blocking collectives, per_device(): resid_full = lax.all_gather(resid_grad, 'tp', axis=1, tiled=True)  6.5 us
  transfers between devices with their start and end apart: 7, of which 5 were waited for; matrix products, arithmetic and copies ran while one was open for 19% of the time, Pallas kernels for 0%

commit v1 on v0

--- a/solution.py
+++ b/solution.py
@@ -63,7 +63,10 @@
     summed = lax.psum_scatter(
         jnp.stack(partials).astype(jnp.bfloat16), "tp", scatter_dimension=2, tiled=True
     )
-    returned = lax.all_to_all(summed, "sp", split_axis=1, concat_axis=0, tiled=True)
+    returned = jnp.concatenate(
+        lax.all_to_all(jnp.stack(jnp.split(summed, lax.axis_size("sp"), axis=1)), "sp", 0, 0),
+        axis=0,
+    )
     return (returned, (jnp.stack(gate_list), jnp.stack(up_list), jnp.stack(down_list)))
 
 

time: 200 us -> 199 us (level)
  other arithmetic: 8.51 us -> 2.95 us
  local copies, waits for them, and re-layouts: 27.8 us -> 30.7 us
  waiting for transfers between devices: 60.4 us -> 63.3 us
    all_gather x1, waiting for transfers between devices: 0.82 us -> 9.29 us  [per_device(): lax.all_gather(mixed_in, 'sp', axis=0, tiled=True)]
    all_to_all x1, waiting for transfers between devices: 5.67 us -> 0.01 us  [per_device(): lax.all_to_all(resid_full, 'sp', split_axis=1, concat_axis=0, tiled=True)]
    unnamed x1 -> x0, other arithmetic: 5.56 us -> none
    unnamed x35 -> x39, local copies, waits for them, and re-layouts: 18.7 us -> 22.9 us
    reduce_scatter x1 -> x0, local copies, waits for them, and re-layouts: 2.82 us -> none  [expert_pass(): lax.psum_scatter(jnp.stack(partials).astype(jnp.bfloat16), 'tp', scatter_...]
  transfers between devices with their start and end apart: 7 -> 7, of which waited for: 5 -> 4; matrix products, arithmetic and copies ran while one was open for 19% -> 19% of each run, Pallas kernels for 0% -> 0%
where the time goes in v1:
time: 199 us; the launch traced here: 197 us
  waiting for transfers between devices  63.3 us (32%)
  matrix products  43.2 us (22%)
  local copies, waits for them, and re-layouts  30.7 us (15%)
  blocking collectives  28.4 us (14%)
  starting transfers between devices  14.9 us (7%)
  between operations  14 us (7%)
  other arithmetic  2.95 us (1%)
    reduce_scatter x1, waiting for transfers between devices, expert_pass(): lax.psum_scatter(jnp.stack(partials).astype(jnp.bfloat16), 'tp', scatter_...  31.1 us
    unnamed x39, local copies, waits for them, and re-layouts  22.9 us
    all_to_all x1, blocking collectives, expert_pass(): lax.all_to_all(outgoing, 'sp', split_axis=0, concat_axis=1, tiled=True)  21.7 us
    dot_general x5, matrix products, contract_first(): lax.dot_general(left, right, (((0,), (0,)), ((), ())), preferred_element_...  20.8 us
    all_gather x1, waiting for transfers between devices, expert_pass(): routed = lax.all_gather(arrived, 'tp', axis=2, tiled=True)  14 us
    dot_general x3, matrix products, contract_last(): lax.dot_general(left, right, (((1,), (1,)), ((), ())), preferred_element_...  10.6 us
    all_gather x1, waiting for transfers between devices, per_device(): lax.all_gather(mixed_in, 'sp', axis=0, tiled=True)  9.29 us
    all_to_all x1, waiting for transfers between devices, expert_pass(): lax.all_to_all(jnp.stack(jnp.split(summed, lax.axis_size('sp'), axis=1)),...  8.89 us
  transfers between devices with their start and end apart: 7, of which 4 were waited for; matrix products, arithmetic and copies ran while one was open for 19% of the time, Pallas kernels for 0%

profile of v1, /device:TPU:0, one launch (start us, length us, event | category | flops | bytes accessed | tf_op | source)
XLA Modules:
  0.0 197.4 jit_solution(2162120262785751519)
XLA Ops:
  7.2 0.0 copy-start
  7.2 0.0 all-gather.3.cloned.1.call-start
  7.2 0.9 copy.41
  8.2 0.1 eq.50
  8.3 0.1 eq.46
  8.5 0.6 reduce-window.6
  9.0 0.2 slice_reduce_fusion
  9.3 0.1 fusion.45
  9.4 1.8 mul.130
  11.2 2.2 %mul.131 = f32[256,512]{1,0:T(8,128)} reshape(f32[128,2,512]{2,1,0:T(2,128)} %mul.130) | data formatting | bytes 1048576 | tf_op jit(solution)/shard_map/mul | solution.py:103
  13.4 0.8 copy.44
  14.2 0.1 mul.128
  14.4 1.4 convolution_convert_fusion
  15.8 21.7 %all_to_all.36 = bf16[8,64,512]{2,1,0:T(8,128)(2,1)} all-to-all(bf16[8,64,512]{2,1,0:T(8,128)(2,1)S(1)} %bitcast.113), channel_id=1, replica_groups=mesh['sp'=8,'tp'=4] {'sp'}, dimensions={0} | all-to-all | bytes 1048576 | tf_op jit(solution)/shard_map/all_to_all | solution.py:54
  37.5 0.0 all-gather.3.cloned.1.call-update
  37.6 0.0 reduce-scatter.2.cloned.1.call-start
  37.6 0.0 copy-start.9
  37.6 0.0 copy-start.11
  37.6 4.7 %fusion.2 = f32[512,768]{1,0:T(8,128)} fusion(bf16[1,2048,768]{2,1,0:T(8,128)(2,1)S(1)} %copy-done, bf16[1,512,2048]{2,1,0:T(8,128)(2,1)} %param.16), kind=kOutput, calls=%fused_computation.6 | convolution fusion | flops 1610612736 | bytes 6815744 | tf_op jit(solution)/shard_map/dot_general | solution.py:34
  42.3 3.0 %fusion.6 = f32[512,768]{1,0:T(8,128)} fusion(bf16[1,2048,768]{2,1,0:T(8,128)(2,1)S(1)} %copy-done.9, bf16[1,512,2048]{2,1,0:T(8,128)(2,1)S(1)} %copy-done.11), kind=kOutput, calls=%fused_computation.10 | convolution fusion | flops 1610612736 | bytes 6815744 | tf_op jit(solution)/shard_map/dot_general | solution.py:35
  45.3 14.0 %all-gather.3.cloned.1.call-done = bf16[1,512,2048]{2,1,0:T(8,128)(2,1)} async-done(((bf16[1,512,512]{2,1,0:T(8,128)(2,1)}), bf16[1,512,2048]{2,1,0:T(8,128)(2,1)}) %all-gather.3.cloned.1.call-update) | async-done | bytes 2097168 | tf_op jit(solution)/shard_map/all_gather | solution.py:55
  59.3 5.6 %multiply_convert_fusion.4 = (bf16[512,768]{1,0:T(8,128)(2,1)S(1)}, bf16[512,768]{1,0:T(8,128)(2,1)S(1)}) fusion(f32[512,768]{1,0:T(8,128)} %fusion.2, f32[512,768]{1,0:T(8,128)} %fusion.6, bf16[1,768,2048]{2,1,0:T(8,128)(2,1)} %param.19, bf16[1,512,2048]{2,1,0:T(8,128)(2,1)} %all-gather.3.cloned.1.call-done), kind=kOutput, calls=%fused_computation.25 | convolution fusion | flops 1615724544 | bytes 9961472 | tf_op jit(solution)/shard_map/dot_general | solution.py:28
  64.9 0.0 copy-start.10
  65.0 1.8 fusion
  66.8 0.6 copy-done.10
  67.4 3.1 %fusion.15 = bf16[1,512,2048]{2,1,0:T(8,128)(2,1)} fusion(f32[512,2048]{1,0:T(8,128)S(1)} %fusion, bf16[512,768]{1,0:T(8,128)(2,1)S(1)} %get-tuple-element.42, bf16[1,2048,768]{2,1,0:T(8,128)(2,1)S(1)} %copy-done.10), kind=kOutput, calls=%fused_computation.17 | convolution fusion | flops 1612709888 | bytes 10223616 | tf_op jit(solution)/shard_map/dot_general | solution.py:28
  70.6 0.0 reduce-scatter.2.cloned.1.call-update
  70.6 0.1 reduce_sum.24
  70.7 0.1 copy.43
  70.8 31.1 %reduce-scatter.2.cloned.1.call-done = bf16[1,512,512]{2,1,0:T(8,128)(2,1)} async-done(((bf16[1,512,2048]{2,1,0:T(8,128)(2,1)}), bf16[1,512,512]{2,1,0:T(8,128)(2,1)}) %reduce-scatter.2.cloned.1.call-update) | async-done | bytes 524304 | tf_op jit(solution)/shard_map/reduce_scatter | solution.py:63
  101.9 1.5 fusion.43
  103.4 1.5 fusion.42
  104.8 1.5 fusion.41
  106.3 1.5 fusion.40
  107.8 1.5 fusion.39
  109.2 1.5 fusion.38
  110.7 1.5 fusion.37
  112.2 1.5 fusion.36
  113.7 5.5 %all-to-all-start.1 = ((bf16[8,1,64,512]{3,2,1,0:T(8,128)(2,1)}), bf16[8,1,64,512]{3,2,1,0:T(8,128)(2,1)}, u32[]{:S(2)}, u32[]{:S(2)}) async-start(bf16[8,1,64,512]{3,2,1,0:T(8,128)(2,1)} %fusion.36), calls=%async_computation.2 | async-start | bytes 1048576 | tf_op jit(solution)/shard_map/all_to_all | solution.py:67
  119.2 0.0 all-gather.5.cloned.1.call-start
  119.2 0.1 fusion.31
  119.3 0.0 copy-start.3
  119.4 5.4 %fusion.10 = bf16[1,2048,768]{1,2,0:T(8,128)(2,1)} fusion(bf16[512,768]{1,0:T(8,128)(2,1)} %copy-done.13, bf16[1,512,2048]{2,1,0:T(8,128)(2,1)} %param.16), kind=kOutput, calls=%fused_computation.14 | convolution fusion | flops 1613758464 | bytes 6029312 | tf_op jit(solution)/shard_map/dot_general | solution.py:22
  124.7 8.9 %all-to-all-done.1 = bf16[8,1,64,512]{3,2,1,0:T(8,128)(2,1)} async-done(((bf16[8,1,64,512]{3,2,1,0:T(8,128)(2,1)}), bf16[8,1,64,512]{3,2,1,0:T(8,128)(2,1)}, u32[]{:S(2)}, u32[]{:S(2)}) %all-to-all-start.1) | async-done | bytes 524320 | tf_op jit(solution)/shard_map/all_to_all | solution.py:67
  133.6 1.3 fusion.25
  134.9 0.0 copy-start.4
  134.9 6.7 %all_gather.10 = bf16[128,2048]{1,0:T(8,128)(2,1)S(1)} all-gather(bf16[128,512]{1,0:T(8,128)(2,1)S(1)} %fusion.25), channel_id=1, replica_groups=mesh['sp'=8,'tp'=4] {'tp'}, dimensions={1}, use_global_device_ids=true | all-gather | bytes 655360 | tf_op jit(solution)/shard_map/all_gather | solution.py:117
  141.6 0.8 copy-done.1
  142.4 2.8 %fusion.29 = (bf16[128,512]{1,0:T(8,128)(2,1)S(1)}, bf16[128,512]{1,0:T(8,128)(2,1)}, bf16[128,512]{1,0:T(8,128)(2,1)}) fusion(bf16[128,512]{1,0:T(8,128)(2,1)} %param.20, bf16[128,512]{1,0:T(8,128)(2,1)} %param.23, bf16[128,2048]{1,0:T(8,128)(2,1)S(1)} %all_gather.10, bf16[2048,512]{1,0:T(8,128)(2,1)} %param.25), kind=kOutput, calls=%fused_computation.42 | convolution fusion | flops 268959744 | bytes 3276800 | tf_op jit(solution)/shard_map/dot_general | solution.py:118
  145.2 0.0 all-gather.5.cloned.1.call-update
  145.2 6.1 %fusion.12 = bf16[1,768,2048]{2,1,0:T(8,128)(2,1)} fusion(bf16[1,512,2048]{2,1,0:T(8,128)(2,1)} %all-gather.3.cloned.1.call-done, f32[512,768]{1,0:T(8,128)} %fusion.6, f32[512,768]{1,0:T(8,128)} %fusion.2), kind=kOutput, calls=%fused_computation.16 | convolution fusion | flops 1616117760 | bytes 8388608 | tf_op jit(solution)/shard_map/dot_general | solution.py:22
  151.4 0.8 copy.50
  152.2 4.2 %all-to-all-start.2 = ((bf16[128,8,256]{2,0,1:T(8,128)(2,1)}), bf16[128,8,256]{2,0,1:T(8,128)(2,1)}, u32[]{:S(2)}, u32[]{:S(2)}) async-start(bf16[128,8,256]{2,0,1:T(8,128)(2,1)} %bitcast.111), calls=%async_computation.3 | async-start | bytes 1048576 | tf_op jit(solution)/shard_map/all_to_all | solution.py:130
  156.4 0.6 fusion.49
  157.0 3.8 %collective-permute-start = (bf16[1,512]{1,0:T(2,128)(2,1)}, bf16[1,512]{1,0:T(2,128)(2,1)S(1)}, u32[]{:S(2)}, u32[]{:S(2)}) collective-permute-start(bf16[1,512]{1,0:T(2,128)(2,1)} %get-tuple-element.47), channel_id=1, source_target_pairs={{0,4},{4,8},{8,12},{12,16},{16,20},{20,24},{24,28},{1,5},{5,9},{9,... | collective-permute-start | bytes 3080 | tf_op jit(solution)/shard_map/ppermute | solution.py:15
  160.7 1.3 collective-permute-start.1
  162.0 5.3 %fusion.11 = bf16[1,2048,768]{1,2,0:T(8,128)(2,1)} fusion(bf16[512,768]{1,0:T(8,128)(2,1)} %copy-done.12, bf16[1,512,2048]{2,1,0:T(8,128)(2,1)} %param.16), kind=kOutput, calls=%fused_computation.15 | convolution fusion | flops 1613758464 | bytes 6029312 | tf_op jit(solution)/shard_map/dot_general | solution.py:22
  167.4 4.6 %copy.46 = bf16[1,2048,768]{2,1,0:T(8,128)(2,1)} copy(bf16[1,2048,768]{1,2,0:T(8,128)(2,1)} %fusion.10) | data formatting | bytes 6291456
  172.0 4.8 %copy.47 = bf16[1,2048,768]{2,1,0:T(8,128)(2,1)} copy(bf16[1,2048,768]{1,2,0:T(8,128)(2,1)} %fusion.11) | data formatting | bytes 6291456
  176.8 0.7 maximum_convert_fusion
  177.5 0.8 multiply_convert_fusion.9
  178.3 0.7 multiply_convert_fusion.10
  179.0 9.3 %all-gather.5.cloned.1.call-done = bf16[1024,512]{1,0:T(8,128)(2,1)} async-done(((bf16[128,512]{1,0:T(8,128)(2,1)}), bf16[1024,512]{1,0:T(8,128)(2,1)}) %all-gather.5.cloned.1.call-update) | async-done | bytes 1048592 | tf_op jit(solution)/shard_map/all_gather | solution.py:131
  188.3 2.6 %convolution_multiply_fusion = f32[256,512]{1,0:T(8,128)} fusion(bf16[1024,256]{1,0:T(8,128)(2,1)} %bitcast.23, bf16[1024,512]{1,0:T(8,128)(2,1)} %all-gather.5.cloned.1.call-done), kind=kOutput, calls=%fused_computation.30 | convolution fusion | flops 268566528 | bytes 2097152 | tf_op jit(solution)/shard_map/dot_general | solution.py:22
  (29 shorter events, 0.1 us)
Async XLA Ops:
  7.2 30.4 %copy-start = (bf16[1,2048,768]{2,1,0:T(8,128)(2,1)S(1)}, bf16[1,2048,768]{2,1,0:T(8,128)(2,1)}, u32[]{:S(2)}) copy-start(bf16[1,2048,768]{2,1,0:T(8,128)(2,1)} %param.17) | copy-start | bytes 9437188
  7.2 52.1 %all-gather.3.cloned.1.call-start = ((), (), s32[]{:S(2)}) async-start(), calls=%async_computation.4 | async-start | bytes 2621440 | tf_op jit(solution)/shard_map/all_gather | solution.py:55
  37.6 64.3 %reduce-scatter.2.cloned.1.call-start = ((), (), s32[]{:S(2)}) async-start(), calls=%async_computation.5 | async-start | bytes 2621440 | tf_op jit(solution)/shard_map/reduce_scatter | solution.py:63
  37.6 4.7 %copy-start.9 = (bf16[1,2048,768]{2,1,0:T(8,128)(2,1)S(1)}, bf16[1,2048,768]{2,1,0:T(8,128)(2,1)}, u32[]{:S(2)}) copy-start(bf16[1,2048,768]{2,1,0:T(8,128)(2,1)} %param.18) | copy-start | bytes 9437188
  37.6 4.7 %copy-start.11 = (bf16[1,512,2048]{2,1,0:T(8,128)(2,1)S(1)}, bf16[1,512,2048]{2,1,0:T(8,128)(2,1)}, u32[]{:S(2)}) copy-start(bf16[1,512,2048]{2,1,0:T(8,128)(2,1)} %param.16) | copy-start | bytes 6291460
  64.9 1.9 copy-start.13
  64.9 1.9 copy-start.12
  64.9 2.5 %copy-start.10 = (bf16[1,2048,768]{2,1,0:T(8,128)(2,1)S(1)}, bf16[1,2048,768]{2,1,0:T(8,128)(2,1)}, u32[]{:S(2)}) copy-start(bf16[1,2048,768]{2,1,0:T(8,128)(2,1)} %param.18) | copy-start | bytes 9437188
  70.5 48.7 %copy-start.8 = (s32[128,2]{0,1:T(2,128)S(1)}, s32[128,2]{0,1:T(2,128)}, u32[]{:S(2)}) copy-start(s32[128,2]{0,1:T(2,128)} %param.14) | copy-start | bytes 3076
  70.5 48.8 %copy-start.7 = (bf16[3,512]{1,0:T(4,128)(2,1)S(1)}, bf16[3,512]{1,0:T(4,128)(2,1)}, u32[]{:S(2)}) copy-start(bf16[3,512]{1,0:T(4,128)(2,1)} %param.24) | copy-start | bytes 9220
  113.7 19.9 %all-to-all-start.1 = ((bf16[8,1,64,512]{3,2,1,0:T(8,128)(2,1)}), bf16[8,1,64,512]{3,2,1,0:T(8,128)(2,1)}, u32[]{:S(2)}, u32[]{:S(2)}) async-start(bf16[8,1,64,512]{3,2,1,0:T(8,128)(2,1)} %fusion.36), calls=%async_computation.2 | async-start | bytes 1048576 | tf_op jit(solution)/shard_map/all_to_all | solution.py:67
  119.2 69.1 %all-gather.5.cloned.1.call-start = ((), (), s32[]{:S(2)}) async-start(), calls=%async_computation.6 | async-start | bytes 1179648 | tf_op jit(solution)/shard_map/all_gather | solution.py:131
  119.3 14.3 %copy-start.3 = (bf16[128,512]{1,0:T(8,128)(2,1)S(1)}, bf16[128,512]{1,0:T(8,128)(2,1)}, u32[]{:S(2)}) copy-start(bf16[128,512]{1,0:T(8,128)(2,1)} %param.13) | copy-start | bytes 393220
  134.9 16.5 %copy-start.4 = (bf16[128,512]{1,0:T(8,128)(2,1)}, bf16[128,512]{1,0:T(8,128)(2,1)S(1)}, u32[]{:S(2)}) copy-start(bf16[128,512]{1,0:T(8,128)(2,1)S(1)} %fusion.25) | copy-start | bytes 393220
  141.6 0.8 copy-start.1
  145.2 6.2 %copy-start.2 = (bf16[128,2048]{1,0:T(8,128)(2,1)S(1)}, bf16[128,2048]{1,0:T(8,128)(2,1)}, u32[]{:S(2)}) copy-start(bf16[128,2048]{1,0:T(8,128)(2,1)} %copy-done.1) | copy-start | bytes 1572868
  152.2 26.8 %all-to-all-start.2 = ((bf16[128,8,256]{2,0,1:T(8,128)(2,1)}), bf16[128,8,256]{2,0,1:T(8,128)(2,1)}, u32[]{:S(2)}, u32[]{:S(2)}) async-start(bf16[128,8,256]{2,0,1:T(8,128)(2,1)} %bitcast.111), calls=%async_computation.3 | async-start | bytes 1048576 | tf_op jit(solution)/shard_map/all_to_all | solution.py:130
  157.0 19.9 %collective-permute-start = (bf16[1,512]{1,0:T(2,128)(2,1)}, bf16[1,512]{1,0:T(2,128)(2,1)S(1)}, u32[]{:S(2)}, u32[]{:S(2)}) collective-permute-start(bf16[1,512]{1,0:T(2,128)(2,1)} %get-tuple-element.47), channel_id=1, source_target_pairs={{0,4},{4,8},{8,12},{12,16},{16,20},{20,24},{24,28},{1,5},{5,9},{9,... | collective-permute-start | bytes 3080 | tf_op jit(solution)/shard_map/ppermute | solution.py:15
  160.7 16.1 %collective-permute-start.1 = (bf16[1,512]{1,0:T(2,128)(2,1)}, bf16[1,512]{1,0:T(2,128)(2,1)}, u32[]{:S(2)}, u32[]{:S(2)}) collective-permute-start(bf16[1,512]{1,0:T(2,128)(2,1)} %get-tuple-element.48), channel_id=1, source_target_pairs={{4,0},{8,4},{12,8},{16,12},{20,16},{24,20},{28,24},{5,1},{9,5},{13... | collective-permute-start | bytes 3080 | tf_op jit(solution)/shard_map/ppermute | solution.py:16
  172.0 5.5 %copy-start.5 = (bf16[128,512]{1,0:T(8,128)(2,1)S(1)}, bf16[128,512]{1,0:T(8,128)(2,1)}, u32[]{:S(2)}) copy-start(bf16[128,512]{1,0:T(8,128)(2,1)} %param.21) | copy-start | bytes 393220
  172.0 6.3 %copy-start.6 = (bf16[128,512]{1,0:T(8,128)(2,1)S(1)}, bf16[128,512]{1,0:T(8,128)(2,1)}, u32[]{:S(2)}) copy-start(bf16[128,512]{1,0:T(8,128)(2,1)} %param.22) | copy-start | bytes 393220
Sparse Core Ops, SparseCore 0:
  37.7 21.5 all-gather.2
  70.7 31.1 reduce-scatter.1
  145.3 42.8 all-gather.4
